TPU v7x, 32 devices: a whole 2x2x4 slice. The times are simulated.
32 devices in a mesh: gr: 2 (over x), fs: 8 (over z, y), tp: 2 (over core).
Axes of the slice: x: 2, y: 2, z: 4, core: 2. Of those that a mesh axis runs over, the one named last changes fastest.
Arguments:
- tokens: bfloat16 [16384, 3072], P(('gr', 'fs')), may hold values from -6 to 6
- norm_gain: float32 [3072], P(('gr', 'fs')), may hold values from 0.1 to 1.9
- gate_weight: float32 [8, 3072, 768], P(None, ('gr', 'fs'), 'tp'), may hold values from -0.109375 to 0.109375
- up_weight: float32 [8, 3072, 768], P(None, ('gr', 'fs'), 'tp'), may hold values from -0.109375 to 0.109375
- down_weight: float32 [8, 3072, 768], P(None, ('gr', 'fs'), 'tp'), may hold values from -0.21875 to 0.21875
- group_pick: int32 [16384], P(('gr', 'fs')), may hold values from 0 to 3, as said below
- expert_pick: int32 [16384, 2], P(('gr', 'fs')), may hold values from 0 to 1, as said below
- route_weight: float32 [16384, 2], P(('gr', 'fs')), may hold values from 0.1 to 1
Outputs:
- combined: bfloat16 [16384, 3072], P(('gr', 'fs'), 'tp')
- gate_served: bfloat16 [8, 3072, 768], P('fs', None, 'tp')
- up_served: bfloat16 [8, 3072, 768], P('fs', None, 'tp')
- down_served: bfloat16 [8, 3072, 768], P('fs', None, 'tp')
Inputs may be any that keep to these rules, and one draw needn't show every extreme that they name: `group_pick`: in each aligned block of 1024 rows every group is picked by the same number of rows. `expert_pick`: the 2 entries of a row differ. In each aligned block of 1024 rows, every expert (group and number together) is named exactly 256 times.
All inputs are finite; a program needn't handle non-finite values.
Results may differ from a plain program's by a relative error of at most 0.0092.
Values may be sent and summed in bfloat16 or wider, within the bound.
A program may use at most 128 MiB of HBM per device.

v0:
```python
import jax
import jax.numpy as jnp
from jax import lax
from jax.sharding import PartitionSpec as P

GROUPS = 4
EPS = 1e-06


def local(
    tokens, norm_gain, gate_weight, up_weight, down_weight, group_pick, expert_pick, route_weight
):
    scaled = norm_gain[None, :, None]
    gate_local = (scaled * gate_weight).astype(jnp.bfloat16)
    up_local = (scaled * up_weight).astype(jnp.bfloat16)
    down_local = down_weight.astype(jnp.bfloat16)
    experts, rows_dev, cols_dev = gate_local.shape
    gate_four = gate_local.reshape(experts, 1, rows_dev, cols_dev)
    up_four = up_local.reshape(experts, 1, rows_dev, cols_dev)
    down_four = down_local.reshape(experts, 1, rows_dev, cols_dev)
    gathered = (
        lax.all_gather(gate_four, "gr", axis=1, tiled=True),
        lax.all_gather(up_four, "gr", axis=1, tiled=True),
        lax.all_gather(down_four, "gr", axis=1, tiled=True),
    )
    relaid = (
        lax.all_to_all(gathered[0], "fs", split_axis=0, concat_axis=2, tiled=True),
        lax.all_to_all(gathered[1], "fs", split_axis=0, concat_axis=2, tiled=True),
        lax.all_to_all(gathered[2], "fs", split_axis=0, concat_axis=2, tiled=True),
    )
    gate_new = relaid[0].reshape(1, -1, cols_dev)
    up_new = relaid[1].reshape(1, -1, cols_dev)
    down_new = relaid[2].reshape(1, -1, cols_dev)
    tok_rows, model_width = tokens.shape
    as_float = tokens.astype(jnp.float32)
    normed = (
        as_float * lax.rsqrt(jnp.mean(as_float * as_float, axis=-1, keepdims=True) + EPS)
    ).astype(jnp.bfloat16)
    per_group = experts // GROUPS
    top_count = expert_pick.shape[1]
    capacity = top_count * tok_rows // experts
    flat_ids = (group_pick[:, None] * per_group + expert_pick).reshape(-1)
    onehot = (flat_ids[:, None] == jnp.arange(experts, dtype=jnp.int32)[None, :]).astype(jnp.int32)
    slot_index = jnp.sum(onehot * (jnp.cumsum(onehot, axis=0) - 1), axis=1)
    target = flat_ids * capacity + slot_index
    source = (
        jnp.zeros((experts * capacity,), jnp.int32)
        .at[target]
        .set(jnp.arange(top_count * tok_rows, dtype=jnp.int32) // top_count)
    )
    outgoing = normed[source].reshape(experts, capacity, model_width)
    share = capacity // lax.axis_size("tp")
    start = lax.axis_index("tp") * share
    my_share = lax.dynamic_slice_in_dim(outgoing, start, share, 1)
    landed = lax.all_to_all(my_share, "fs", split_axis=0, concat_axis=1, tiled=True).reshape(
        experts, share, model_width
    )
    arrived = lax.all_gather(landed, "tp", axis=1, tiled=True).reshape(-1, model_width)
    gate_acts = jnp.dot(arrived, gate_new[0], preferred_element_type=jnp.float32)
    up_acts = jnp.dot(arrived, up_new[0], preferred_element_type=jnp.float32)
    hidden = (jax.nn.silu(gate_acts) * up_acts).astype(jnp.bfloat16)
    partial_value = lax.dot_general(
        hidden, down_new[0], (((1,), (1,)), ((), ())), preferred_element_type=jnp.float32
    ).astype(jnp.bfloat16)
    summed = (
        lax.psum_scatter(partial_value, "tp", scatter_dimension=1, tiled=True)
        .astype(jnp.float32)
        .astype(jnp.bfloat16)
    )
    returned = lax.all_to_all(summed, "fs", split_axis=0, concat_axis=0, tiled=True)
    picked = returned[target].reshape(tok_rows, top_count, -1).astype(jnp.float32)
    combined = jnp.sum(route_weight[:, :, None] * picked, axis=1).astype(jnp.bfloat16)
    return (combined, gate_new, up_new, down_new)


def solution(mesh):
    in_specs = (
        P(("gr", "fs"), None),
        P(("gr", "fs")),
        P(None, ("gr", "fs"), "tp"),
        P(None, ("gr", "fs"), "tp"),
        P(None, ("gr", "fs"), "tp"),
        P(("gr", "fs")),
        P(("gr", "fs"), None),
        P(("gr", "fs"), None),
    )
    out_specs = (
        P(("gr", "fs"), "tp"),
        P("fs", None, "tp"),
        P("fs", None, "tp"),
        P("fs", None, "tp"),
    )
    return jax.shard_map(local, mesh=mesh, in_specs=in_specs, out_specs=out_specs, check_vma=False)
```

profile of v0, /device:TPU:0, one launch (start us, length us, event | category | flops | bytes accessed | tf_op | source)
XLA Modules:
  0.0 640.0 jit_solution(4031025524227223699)
XLA Ops:
  12.8 8.0 %scatter_custom_fusion = s32[2048]{0:T(1024)S(1)} fusion(s32[2048]{0:T(1024)S(1)} %bitcast.62, s32[2048]{0:T(1024)S(1)} %add_select_fusion, s32[]{:T(128)} %constant.39.clone.1), kind=kCustom, calls=%fused_computation.34 | custom fusion | bytes 8196 | tf_op jit(solution)/shard_map/scatter | solution.py:49
  20.9 4.2 fusion
  25.5 5.1 fusion.1
  30.6 26.6 %gather_fusion = bf16[2048,3072]{1,0:T(8,128)(2,1)} fusion(bf16[1024,3072]{1,0:T(8,128)(2,1)} %fusion.1, s32[2048]{0:T(1024)S(1)} %fusion.8), kind=kCustom, calls=%fused_computation | custom fusion | bytes 25174016 | tf_op jit(solution)/shard_map/gather | solution.py:51
  57.2 5.9 constant_dynamic-slice_fusion
  63.1 7.4 %all-to-all-start = ((bf16[8,128,3072]{2,1,0:T(8,128)(2,1)}), bf16[8,128,3072]{2,1,0:T(8,128)(2,1)}, u32[]{:S(2)}, u32[]{:S(2)}) async-start(bf16[8,128,3072]{2,1,0:T(8,128)(2,1)} %constant_dynamic-slice_fusion), calls=%async_computation | async-start | bytes 12582912 | tf_op jit(solution)/shard_map/all_to_all | solution.py:55
  70.6 4.5 multiply_convert_fusion.1
  77.1 131.6 %all-to-all-done = bf16[8,128,3072]{2,1,0:T(8,128)(2,1)} async-done(((bf16[8,128,3072]{2,1,0:T(8,128)(2,1)}), bf16[8,128,3072]{2,1,0:T(8,128)(2,1)}, u32[]{:S(2)}, u32[]{:S(2)}) %all-to-all-start) | async-done | bytes 6291488 | tf_op jit(solution)/shard_map/all_to_all | solution.py:55
  208.8 3.6 all-to-all-start.1
  212.5 54.0 %all-to-all-done.1 = bf16[8,2,192,384]{3,2,1,0:T(8,128)(2,1)S(1)} async-done(((bf16[8,2,192,384]{3,2,1,0:T(8,128)(2,1)}), bf16[8,2,192,384]{3,2,1,0:T(8,128)(2,1)S(1)}, u32[]{:S(2)}, u32[]{:S(2)}) %all-to-all-start.1) | async-done | bytes 2359328 | tf_op jit(solution)/shard_map/all_to_all | solution.py:27
  266.5 4.4 all-to-all-start.2
  270.9 53.4 %all-to-all-done.2 = bf16[8,2,192,384]{3,2,1,0:T(8,128)(2,1)} async-done(((bf16[8,2,192,384]{3,2,1,0:T(8,128)(2,1)}), bf16[8,2,192,384]{3,2,1,0:T(8,128)(2,1)}, u32[]{:S(2)}, u32[]{:S(2)}) %all-to-all-start.2) | async-done | bytes 2359328 | tf_op jit(solution)/shard_map/all_to_all | solution.py:28
  324.3 4.4 all-to-all-start.3
  330.6 3.3 copy.32
  333.9 48.2 %all-to-all-done.3 = bf16[8,2,192,384]{3,2,1,0:T(8,128)(2,1)} async-done(((bf16[8,2,192,384]{3,2,1,0:T(8,128)(2,1)}), bf16[8,2,192,384]{3,2,1,0:T(8,128)(2,1)}, u32[]{:S(2)}, u32[]{:S(2)}) %all-to-all-start.3) | async-done | bytes 2359328 | tf_op jit(solution)/shard_map/all_to_all | solution.py:29
  382.1 3.3 copy.33
  385.4 10.7 %fusion.13 = f32[2048,384]{1,0:T(8,128)} fusion(bf16[2048,3072]{1,0:T(8,128)(2,1)} %bitcast.65, bf16[3072,384]{1,0:T(8,128)(2,1)S(1)} %bitcast.54), kind=kOutput, calls=%fused_computation.40 | convolution fusion | flops 4831838208 | bytes 18087936 | tf_op jit(solution)/shard_map/dot_general | solution.py:59
  396.1 20.7 %convolution_convert_fusion = bf16[2048,3072]{1,0:T(8,128)(2,1)} fusion(bf16[3072,384]{1,0:T(8,128)(2,1)} %bitcast.59, f32[2048,384]{1,0:T(8,128)} %fusion.13, bf16[2048,3072]{1,0:T(8,128)(2,1)} %bitcast.66, bf16[3072,384]{1,0:T(8,128)(2,1)} %bitcast.55), kind=kOutput, calls=%fused_computation.8 | convolution fusion | flops 9674686464 | bytes 33030144 | tf_op jit(solution)/shard_map/dot_general | solution.py:62
  416.9 18.6 %reduce-scatter.2.cloned.1.call-done = bf16[2048,1536]{1,0:T(8,128)(2,1)} async-done(((bf16[2048,3072]{1,0:T(8,128)(2,1)}), bf16[2048,1536]{1,0:T(8,128)(2,1)}) %reduce-scatter.2.cloned.1.call-update) | async-done | bytes 6291472 | tf_op jit(solution)/shard_map/reduce_scatter | solution.py:66
  435.5 6.0 all-to-all-start.4
  441.7 138.3 %all-to-all-done.4 = bf16[8,256,1536]{2,1,0:T(8,128)(2,1)} async-done(((bf16[8,256,1536]{2,1,0:T(8,128)(2,1)}), bf16[8,256,1536]{2,1,0:T(8,128)(2,1)}, u32[]{:S(2)}, u32[]{:S(2)}) %all-to-all-start.4) | async-done | bytes 6291488 | tf_op jit(solution)/shard_map/all_to_all | solution.py:70
  580.0 16.9 %gather_fusion.1 = bf16[2048,1536]{1,0:T(8,128)(2,1)} fusion(bf16[2048,1536]{1,0:T(8,128)(2,1)} %bitcast.18, s32[2048]{0:T(1024)S(1)} %broadcast_clamp_fusion), kind=kCustom, calls=%fused_computation.1 | custom fusion | bytes 12591104 | tf_op jit(solution)/shard_map/gather | solution.py:71
  596.9 14.2 %reshape.117 = f32[1024,2,1536]{2,1,0:T(2,128)} reshape(bf16[2048,1536]{1,0:T(8,128)(2,1)} %gather_fusion.1) | data formatting | bytes 18874368 | tf_op jit(solution)/shard_map/convert_element_type | solution.py:71
  611.1 22.4 %multiply_reduce_fusion = bf16[1024,1536]{1,0:T(8,128)(2,1)} fusion(f32[1024,2,1536]{2,1,0:T(2,128)} %reshape.117, f32[1024,2]{1,0:T(8,128)S(1)} %copy.27), kind=kLoop, calls=%fused_computation.7 | loop fusion | flops 4718592 | bytes 15736832 | tf_op jit(solution)/shard_map/reduce_sum | solution.py:72
  (45 shorter events, 10.2 us)
Async XLA Ops:
  20.9 4.6 copy-start
  63.1 7.5 %copy-start.4 = (f32[192]{0:T(256)S(1)}, f32[192]{0:T(256)}, u32[]{:S(2)}) copy-start(f32[192]{0:T(256)} %param.9) | copy-start | bytes 2308
  63.1 145.7 %all-to-all-start = ((bf16[8,128,3072]{2,1,0:T(8,128)(2,1)}), bf16[8,128,3072]{2,1,0:T(8,128)(2,1)}, u32[]{:S(2)}, u32[]{:S(2)}) async-start(bf16[8,128,3072]{2,1,0:T(8,128)(2,1)} %constant_dynamic-slice_fusion), calls=%async_computation | async-start | bytes 12582912 | tf_op jit(solution)/shard_map/all_to_all | solution.py:55
  70.5 5.4 copy-start.1
  70.5 138.3 %all-gather.10.cloned.1.call-start = ((), (), s32[]{:S(2)}) async-start(), calls=%async_computation.8 | async-start | bytes 3538944 | tf_op jit(solution)/shard_map/all_gather | solution.py:22
  75.1 137.4 %all-gather.12.cloned.1.call-start = ((), (), s32[]{:S(2)}) async-start(), calls=%async_computation.9 | async-start | bytes 3538944 | tf_op jit(solution)/shard_map/all_gather | solution.py:23
  75.9 195.0 %all-gather.14.cloned.1.call-start = ((), (), s32[]{:S(2)}) async-start(), calls=%async_computation.10 | async-start | bytes 3538944 | tf_op jit(solution)/shard_map/all_gather | solution.py:24
  77.1 308.3 %all-gather.8.cloned.1.call-start = ((), (), s32[]{:S(2)}) async-start(), calls=%async_computation.6 | async-start | bytes 18874368 | tf_op jit(solution)/shard_map/all_gather | solution.py:58
  208.8 57.7 %all-to-all-start.1 = ((bf16[8,2,192,384]{3,2,1,0:T(8,128)(2,1)}), bf16[8,2,192,384]{3,2,1,0:T(8,128)(2,1)S(1)}, u32[]{:S(2)}, u32[]{:S(2)}) async-start(bf16[8,2,192,384]{3,2,1,0:T(8,128)(2,1)} %bitcast.58), calls=%async_computation.1 | async-start | bytes 4718592 | tf_op jit(solution)/shard_map/all_to_all | solution.py:27
  266.5 57.8 %all-to-all-start.2 = ((bf16[8,2,192,384]{3,2,1,0:T(8,128)(2,1)}), bf16[8,2,192,384]{3,2,1,0:T(8,128)(2,1)}, u32[]{:S(2)}, u32[]{:S(2)}) async-start(bf16[8,2,192,384]{3,2,1,0:T(8,128)(2,1)} %bitcast.57), calls=%async_computation.2 | async-start | bytes 4718592 | tf_op jit(solution)/shard_map/all_to_all | solution.py:28
  324.3 57.8 %all-to-all-start.3 = ((bf16[8,2,192,384]{3,2,1,0:T(8,128)(2,1)}), bf16[8,2,192,384]{3,2,1,0:T(8,128)(2,1)}, u32[]{:S(2)}, u32[]{:S(2)}) async-start(bf16[8,2,192,384]{3,2,1,0:T(8,128)(2,1)} %bitcast.52), calls=%async_computation.3 | async-start | bytes 4718592 | tf_op jit(solution)/shard_map/all_to_all | solution.py:29
  328.7 106.8 %reduce-scatter.2.cloned.1.call-start = ((), (), s32[]{:S(2)}) async-start(), calls=%async_computation.7 | async-start | bytes 18874368 | tf_op jit(solution)/shard_map/reduce_scatter | solution.py:66
  333.9 51.5 %copy-start.2 = (bf16[8,2,192,384]{3,2,0,1:T(8,128)(2,1)S(1)}, bf16[8,2,192,384]{3,2,0,1:T(8,128)(2,1)}, u32[]{:S(2)}) copy-start(bf16[8,2,192,384]{3,2,0,1:T(8,128)(2,1)} %copy.31) | copy-start | bytes 7077892
  435.4 6.0 copy-start.3
  435.5 144.6 %all-to-all-start.4 = ((bf16[8,256,1536]{2,1,0:T(8,128)(2,1)}), bf16[8,256,1536]{2,1,0:T(8,128)(2,1)}, u32[]{:S(2)}, u32[]{:S(2)}) async-start(bf16[8,256,1536]{2,1,0:T(8,128)(2,1)} %bitcast.51), calls=%async_computation.5 | async-start | bytes 12582912 | tf_op jit(solution)/shard_map/all_to_all | solution.py:70
Sparse Core Ops, SparseCore 0:
  75.2 37.3 all-gather.9
  114.8 36.0 all-gather.11
  153.0 36.0 all-gather.13
  208.9 23.5 all-gather.7
  417.0 18.4 reduce-scatter.1
where the time goes:
time: 641 us; the launch traced here: 640 us
  waiting for transfers between devices  445 us (69%)
  local copies, waits for them, and re-layouts  82.1 us (13%)
  other arithmetic  41.4 us (6%)
  matrix products  31.4 us (5%)
  starting transfers between devices  26.3 us (4%)
  between operations  14 us (2%)
    all_to_all x1, waiting for transfers between devices, local(): lax.all_to_all(summed, 'fs', split_axis=0, concat_axis=0, tiled=True)  138 us
    all_to_all x1, waiting for transfers between devices, local(): lax.all_to_all(my_share, 'fs', split_axis=0, concat_axis=1, tiled=True)  132 us
    all_to_all x1, waiting for transfers between devices, local(): lax.all_to_all(gathered[0], 'fs', split_axis=0, concat_axis=2, tiled=True)  54 us
    all_to_all x1, waiting for transfers between devices, local(): lax.all_to_all(gathered[1], 'fs', split_axis=0, concat_axis=2, tiled=True)  53.4 us
    all_to_all x1, waiting for transfers between devices, local(): lax.all_to_all(gathered[2], 'fs', split_axis=0, concat_axis=2, tiled=True)  48.2 us
    gather x1, local copies, waits for them, and re-layouts, local(): outgoing = normed[source].reshape(experts, capacity, model_width)  26.6 us
    reduce_sum x1, other arithmetic, local(): jnp.sum(route_weight[:, :, None] * picked, axis=1).astype(jnp.bfloat16)  22.4 us
    dot_general x1, matrix products, local(): lax.dot_general(hidden, down_new[0], (((1,), (1,)), ((), ())), preferred_...  20.7 us
  transfers between devices with their start and end apart: 10, of which 6 were waited for; matrix products, arithmetic and copies ran while one was open for 2% of the time, Pallas kernels for 0%

commit v1 on v0

--- a/solution.py
+++ b/solution.py
@@ -5,6 +5,22 @@
 
 GROUPS = 4
 EPS = 1e-06
+
+
+def pairwise_exchange(x, axis, split, join):
+    ways, here = (lax.axis_size(axis), lax.axis_index(axis))
+    width = x.shape[split] // ways
+    shape = list(x.shape)
+    shape[split] = width
+    height = shape[join]
+    shape[join] = height * ways
+    full = jnp.zeros(shape, x.dtype)
+    for mask in range(ways):
+        part = lax.dynamic_slice_in_dim(x, (here ^ mask) * width, width, axis=split)
+        if mask:
+            part = lax.ppermute(part, axis, [(d, d ^ mask) for d in range(ways)])
+        full = lax.dynamic_update_slice_in_dim(full, part, (here ^ mask) * height, axis=join)
+    return full
 
 
 def local(
@@ -26,7 +42,7 @@
     relaid = (
         lax.all_to_all(gathered[0], "fs", split_axis=0, concat_axis=2, tiled=True),
         lax.all_to_all(gathered[1], "fs", split_axis=0, concat_axis=2, tiled=True),
-        lax.all_to_all(gathered[2], "fs", split_axis=0, concat_axis=2, tiled=True),
+        pairwise_exchange(gathered[2], "fs", 0, 2),
     )
     gate_new = relaid[0].reshape(1, -1, cols_dev)
     up_new = relaid[1].reshape(1, -1, cols_dev)

time: 641 us -> 636 us (level)
  waiting for transfers between devices: 445 us -> 419 us
  starting transfers between devices: 26.3 us -> 38.7 us
  local copies, waits for them, and re-layouts: 82.1 us -> 91.5 us
    ppermute x0 -> x7, waiting for transfers between devices: none -> 66.4 us  [pairwise_exchange(): part = lax.ppermute(part, axis, [(d, d ^ mask) for d in range(ways)])]
    all_to_all x1, waiting for transfers between devices: 53.4 us -> 0.01 us  [local(): lax.all_to_all(gathered[1], 'fs', split_axis=0, concat_axis=2, tiled=True)]
    all_to_all x1 -> x0, waiting for transfers between devices: 48.2 us -> none  [local(): lax.all_to_all(gathered[2], 'fs', split_axis=0, concat_axis=2, tiled=True)]
    ppermute x0 -> x7, starting transfers between devices: none -> 16.8 us  [pairwise_exchange(): part = lax.ppermute(part, axis, [(d, d ^ mask) for d in range(ways)])]
    reduce_scatter x1, waiting for transfers between devices: 18.6 us -> 27.7 us  [local(): lax.psum_scatter(partial_value, 'tp', scatter_dimension=1, tiled=True)]
    dynamic_update_slice x0 -> x7, local copies, waits for them, and re-layouts: none -> 8.08 us  [pairwise_exchange(): lax.dynamic_update_slice_in_dim(full, part, (here ^ mask) * height, axis=...]
  transfers between devices with their start and end apart: 10 -> 16, of which waited for: 6 -> 9; matrix products, arithmetic and copies ran while one was open for 2% -> 3% of each run, Pallas kernels for 0% -> 0%
where the time goes in v1:
time: 636 us; the launch traced here: 635 us
  waiting for transfers between devices  419 us (66%)
  local copies, waits for them, and re-layouts  91.5 us (14%)
  other arithmetic  40.5 us (6%)
  starting transfers between devices  38.7 us (6%)
  matrix products  31.4 us (5%)
  between operations  14 us (2%)
    all_to_all x1, waiting for transfers between devices, local(): lax.all_to_all(summed, 'fs', split_axis=0, concat_axis=0, tiled=True)  138 us
    all_to_all x1, waiting for transfers between devices, local(): lax.all_to_all(my_share, 'fs', split_axis=0, concat_axis=1, tiled=True)  132 us
    ppermute x7, waiting for transfers between devices, pairwise_exchange(): part = lax.ppermute(part, axis, [(d, d ^ mask) for d in range(ways)])  66.4 us
    all_to_all x1, waiting for transfers between devices, local(): lax.all_to_all(gathered[0], 'fs', split_axis=0, concat_axis=2, tiled=True)  54 us
    reduce_scatter x1, waiting for transfers between devices, local(): lax.psum_scatter(partial_value, 'tp', scatter_dimension=1, tiled=True)  27.7 us
    gather x1, local copies, waits for them, and re-layouts, local(): outgoing = normed[source].reshape(experts, capacity, model_width)  26.6 us
    reduce_sum x1, other arithmetic, local(): jnp.sum(route_weight[:, :, None] * picked, axis=1).astype(jnp.bfloat16)  22.4 us
    dot_general x1, matrix products, local(): lax.dot_general(hidden, down_new[0], (((1,), (1,)), ((), ())), preferred_...  20.7 us
  transfers between devices with their start and end apart: 16, of which 9 were waited for; matrix products, arithmetic and copies ran while one was open for 3% of the time, Pallas kernels for 0%

profile of v1, /device:TPU:0, one launch (start us, length us, event | category | flops | bytes accessed | tf_op | source)
XLA Modules:
  0.0 635.2 jit_solution(11858004120499704359)
XLA Ops:
  12.8 8.0 %scatter_custom_fusion = s32[2048]{0:T(1024)S(1)} fusion(s32[2048]{0:T(1024)S(1)} %bitcast.55, s32[2048]{0:T(1024)S(1)} %add_select_fusion, s32[]{:T(128)} %constant.26.clone.1), kind=kCustom, calls=%fused_computation.50 | custom fusion | bytes 8196 | tf_op jit(solution)/shard_map/scatter | solution.py:65
  20.9 4.2 fusion
  25.5 5.1 fusion.1
  30.6 26.6 %gather_fusion = bf16[2048,3072]{1,0:T(8,128)(2,1)} fusion(bf16[1024,3072]{1,0:T(8,128)(2,1)} %fusion.1, s32[2048]{0:T(1024)S(1)} %fusion.8), kind=kCustom, calls=%fused_computation | custom fusion | bytes 25174016 | tf_op jit(solution)/shard_map/gather | solution.py:67
  57.2 5.9 constant_dynamic-slice_fusion.7
  63.1 7.4 %all-to-all-start = ((bf16[8,128,3072]{2,1,0:T(8,128)(2,1)}), bf16[8,128,3072]{2,1,0:T(8,128)(2,1)}, u32[]{:S(2)}, u32[]{:S(2)}) async-start(bf16[8,128,3072]{2,1,0:T(8,128)(2,1)} %constant_dynamic-slice_fusion.7), calls=%async_computation | async-start | bytes 12582912 | tf_op jit(solution)/shard_map/all_to_all | solution.py:71
  77.1 131.7 %all-to-all-done = bf16[8,128,3072]{2,1,0:T(8,128)(2,1)} async-done(((bf16[8,128,3072]{2,1,0:T(8,128)(2,1)}), bf16[8,128,3072]{2,1,0:T(8,128)(2,1)}, u32[]{:S(2)}, u32[]{:S(2)}) %all-to-all-start) | async-done | bytes 6291488 | tf_op jit(solution)/shard_map/all_to_all | solution.py:71
  208.8 3.6 all-to-all-start.1
  212.5 54.0 %all-to-all-done.1 = bf16[8,2,192,384]{3,2,1,0:T(8,128)(2,1)S(1)} async-done(((bf16[8,2,192,384]{3,2,1,0:T(8,128)(2,1)}), bf16[8,2,192,384]{3,2,1,0:T(8,128)(2,1)S(1)}, u32[]{:S(2)}, u32[]{:S(2)}) %all-to-all-start.1) | async-done | bytes 2359328 | tf_op jit(solution)/shard_map/all_to_all | solution.py:43
  266.5 4.4 all-to-all-start.2
  282.3 15.0 %collective-permute-done = bf16[1,2,192,384]{3,2,1,0:T(8,128)(2,1)} collective-permute-done((bf16[1,2,192,384]{3,2,1,0:T(8,128)(2,1)}, bf16[1,2,192,384]{3,2,1,0:T(8,128)(2,1)}, u32[]{:S(2)}, u32[]{:S(2)}) %collective-permute-start) | collective-permute-done | bytes 294944 | tf_op jit(solution)/shard_map/ppermute | solution.py:21
  297.3 5.5 collective-permute-start.5
  304.5 12.8 %collective-permute-done.1 = bf16[1,2,192,384]{3,2,1,0:T(8,128)(2,1)} collective-permute-done((bf16[1,2,192,384]{3,2,1,0:T(8,128)(2,1)}, bf16[1,2,192,384]{3,2,1,0:T(8,128)(2,1)}, u32[]{:S(2)}, u32[]{:S(2)}) %collective-permute-start.1) | collective-permute-done | bytes 294944 | tf_op jit(solution)/shard_map/ppermute | solution.py:21
  317.3 3.9 collective-permute-start.6
  325.4 32.2 %collective-permute-done.3 = bf16[1,2,192,384]{3,2,1,0:T(8,128)(2,1)S(1)} collective-permute-done((bf16[1,2,192,384]{3,2,1,0:T(8,128)(2,1)S(1)}, bf16[1,2,192,384]{3,2,1,0:T(8,128)(2,1)S(1)}, u32[]{:S(2)}, u32[]{:S(2)}) %collective-permute-start.3) | collective-permute-done | bytes 294944 | tf_op jit(solution)/shard_map/ppermute | solution.py:21
  358.4 5.7 collective-permute-done.4
  371.4 10.7 %fusion.13 = f32[2048,384]{1,0:T(8,128)} fusion(bf16[2048,3072]{1,0:T(8,128)(2,1)} %bitcast.58, bf16[3072,384]{1,0:T(8,128)(2,1)S(1)} %bitcast.50), kind=kOutput, calls=%fused_computation.55 | convolution fusion | flops 4831838208 | bytes 18087936 | tf_op jit(solution)/shard_map/dot_general | solution.py:75
  382.2 20.7 %convolution_convert_fusion = bf16[2048,3072]{1,0:T(8,128)(2,1)} fusion(bf16[3072,384]{1,0:T(8,128)(2,1)} %bitcast.14, f32[2048,384]{1,0:T(8,128)} %fusion.13, bf16[2048,3072]{1,0:T(8,128)(2,1)} %bitcast.59, bf16[3072,384]{1,0:T(8,128)(2,1)} %bitcast.52), kind=kOutput, calls=%fused_computation.8 | convolution fusion | flops 9674686464 | bytes 33030144 | tf_op jit(solution)/shard_map/dot_general | solution.py:78
  402.9 27.7 %reduce-scatter.2.cloned.1.call-done = bf16[2048,1536]{1,0:T(8,128)(2,1)} async-done(((bf16[2048,3072]{1,0:T(8,128)(2,1)}), bf16[2048,1536]{1,0:T(8,128)(2,1)}) %reduce-scatter.2.cloned.1.call-update) | async-done | bytes 6291472 | tf_op jit(solution)/shard_map/reduce_scatter | solution.py:82
  430.6 6.0 all-to-all-start.3
  436.9 138.3 %all-to-all-done.3 = bf16[8,256,1536]{2,1,0:T(8,128)(2,1)} async-done(((bf16[8,256,1536]{2,1,0:T(8,128)(2,1)}), bf16[8,256,1536]{2,1,0:T(8,128)(2,1)}, u32[]{:S(2)}, u32[]{:S(2)}) %all-to-all-start.3) | async-done | bytes 6291488 | tf_op jit(solution)/shard_map/all_to_all | solution.py:86
  575.2 16.9 %gather_fusion.1 = bf16[2048,1536]{1,0:T(8,128)(2,1)} fusion(bf16[2048,1536]{1,0:T(8,128)(2,1)} %bitcast.16, s32[2048]{0:T(1024)S(1)} %broadcast_clamp_fusion), kind=kCustom, calls=%fused_computation.1 | custom fusion | bytes 12591104 | tf_op jit(solution)/shard_map/gather | solution.py:87
  592.1 14.2 %reshape.115 = f32[1024,2,1536]{2,1,0:T(2,128)} reshape(bf16[2048,1536]{1,0:T(8,128)(2,1)} %gather_fusion.1) | data formatting | bytes 18874368 | tf_op jit(solution)/shard_map/convert_element_type | solution.py:87
  606.3 22.4 %multiply_reduce_fusion = bf16[1024,1536]{1,0:T(8,128)(2,1)} fusion(f32[1024,2,1536]{2,1,0:T(2,128)} %reshape.115, f32[1024,2]{1,0:T(8,128)S(1)} %copy.25), kind=kLoop, calls=%fused_computation.7 | loop fusion | flops 4718592 | bytes 15736832 | tf_op jit(solution)/shard_map/reduce_sum | solution.py:88
  (69 shorter events, 38.1 us)
Async XLA Ops:
  20.9 4.6 copy-start
  63.1 7.5 %copy-start.4 = (f32[8,192,384]{2,1,0:T(8,128)S(1)}, f32[8,192,384]{2,1,0:T(8,128)}, u32[]{:S(2)}) copy-start(f32[8,192,384]{2,1,0:T(8,128)} %param.11) | copy-start | bytes 7077892
  63.1 7.5 %copy-start.6 = (f32[192]{0:T(256)S(1)}, f32[192]{0:T(256)}, u32[]{:S(2)}) copy-start(f32[192]{0:T(256)} %param.9) | copy-start | bytes 2308
  63.1 145.7 %all-to-all-start = ((bf16[8,128,3072]{2,1,0:T(8,128)(2,1)}), bf16[8,128,3072]{2,1,0:T(8,128)(2,1)}, u32[]{:S(2)}, u32[]{:S(2)}) async-start(bf16[8,128,3072]{2,1,0:T(8,128)(2,1)} %constant_dynamic-slice_fusion.7), calls=%async_computation | async-start | bytes 12582912 | tf_op jit(solution)/shard_map/all_to_all | solution.py:71
  70.5 138.3 %all-gather.10.cloned.1.call-start = ((), (), s32[]{:S(2)}) async-start(), calls=%async_computation.7 | async-start | bytes 3538944 | tf_op jit(solution)/shard_map/all_gather | solution.py:38
  74.2 1.7 copy-start.1
  74.2 138.2 %all-gather.12.cloned.1.call-start = ((), (), s32[]{:S(2)}) async-start(), calls=%async_computation.8 | async-start | bytes 3538944 | tf_op jit(solution)/shard_map/all_gather | solution.py:39
  75.0 196.2 %all-gather.14.cloned.1.call-start = ((), (), s32[]{:S(2)}) async-start(), calls=%async_computation.9 | async-start | bytes 3538944 | tf_op jit(solution)/shard_map/all_gather | solution.py:40
  77.1 294.3 %all-gather.8.cloned.1.call-start = ((), (), s32[]{:S(2)}) async-start(), calls=%async_computation.5 | async-start | bytes 18874368 | tf_op jit(solution)/shard_map/all_gather | solution.py:74
  208.8 57.7 %all-to-all-start.1 = ((bf16[8,2,192,384]{3,2,1,0:T(8,128)(2,1)}), bf16[8,2,192,384]{3,2,1,0:T(8,128)(2,1)S(1)}, u32[]{:S(2)}, u32[]{:S(2)}) async-start(bf16[8,2,192,384]{3,2,1,0:T(8,128)(2,1)} %bitcast.51), calls=%async_computation.1 | async-start | bytes 4718592 | tf_op jit(solution)/shard_map/all_to_all | solution.py:43
  266.5 101.4 %all-to-all-start.2 = ((bf16[8,2,192,384]{3,2,1,0:T(8,128)(2,1)}), bf16[8,2,192,384]{3,2,1,0:T(8,128)(2,1)}, u32[]{:S(2)}, u32[]{:S(2)}) async-start(bf16[8,2,192,384]{3,2,1,0:T(8,128)(2,1)} %bitcast.47), calls=%async_computation.2 | async-start | bytes 4718592 | tf_op jit(solution)/shard_map/all_to_all | solution.py:44
  270.9 159.7 %reduce-scatter.2.cloned.1.call-start = ((), (), s32[]{:S(2)}) async-start(), calls=%async_computation.6 | async-start | bytes 18874368 | tf_op jit(solution)/shard_map/reduce_scatter | solution.py:82
  271.2 2.5 copy-start.2
  274.9 22.4 %collective-permute-start = (bf16[1,2,192,384]{3,2,1,0:T(8,128)(2,1)}, bf16[1,2,192,384]{3,2,1,0:T(8,128)(2,1)}, u32[]{:S(2)}, u32[]{:S(2)}) collective-permute-start(bf16[1,2,192,384]{3,2,1,0:T(8,128)(2,1)} %get-tuple-element.12), channel_id=1, source_target_pairs={{0,2},{2,0},{4,6},{6,4},{8,10},{10,8},{12,14},{14,12},{1,3},{3,1},... | collective-permute-start | bytes 884744 | tf_op jit(solution)/shard_map/ppermute | solution.py:21
  276.5 40.9 %collective-permute-start.1 = (bf16[1,2,192,384]{3,2,1,0:T(8,128)(2,1)}, bf16[1,2,192,384]{3,2,1,0:T(8,128)(2,1)}, u32[]{:S(2)}, u32[]{:S(2)}) collective-permute-start(bf16[1,2,192,384]{3,2,1,0:T(8,128)(2,1)} %get-tuple-element.11), channel_id=1, source_target_pairs={{0,4},{2,6},{4,0},{6,2},{8,12},{10,14},{12,8},{14,10},{1,5},{3,7},... | collective-permute-start | bytes 884744 | tf_op jit(solution)/shard_map/ppermute | solution.py:21
  278.0 45.7 %collective-permute-start.2 = (bf16[1,2,192,384]{3,2,1,0:T(8,128)(2,1)}, bf16[1,2,192,384]{3,2,1,0:T(8,128)(2,1)}, u32[]{:S(2)}, u32[]{:S(2)}) collective-permute-start(bf16[1,2,192,384]{3,2,1,0:T(8,128)(2,1)} %get-tuple-element.10), channel_id=1, source_target_pairs={{0,6},{2,4},{4,2},{6,0},{8,14},{10,12},{12,10},{14,8},{1,7},{3,5},... | collective-permute-start | bytes 884744 | tf_op jit(solution)/shard_map/ppermute | solution.py:21
  278.4 79.2 %collective-permute-start.3 = (bf16[1,2,192,384]{3,2,1,0:T(8,128)(2,1)S(1)}, bf16[1,2,192,384]{3,2,1,0:T(8,128)(2,1)S(1)}, u32[]{:S(2)}, u32[]{:S(2)}) collective-permute-start(bf16[1,2,192,384]{3,2,1,0:T(8,128)(2,1)S(1)} %get-tuple-element.9), channel_id=1, source_target_pairs={{0,8},{2,10},{4,12},{6,14},{8,0},{10,2},{12,4},{14,6},{1,9},{3,11}... | collective-permute-start | bytes 884744 | tf_op jit(solution)/shard_map/ppermute | solution.py:21
  280.9 83.1 %collective-permute-start.4 = (bf16[1,2,192,384]{3,2,1,0:T(8,128)(2,1)S(1)}, bf16[1,2,192,384]{3,2,1,0:T(8,128)(2,1)S(1)}, u32[]{:S(2)}, u32[]{:S(2)}) collective-permute-start(bf16[1,2,192,384]{3,2,1,0:T(8,128)(2,1)S(1)} %get-tuple-element.8), channel_id=1, source_target_pairs={{0,10},{2,8},{4,14},{6,12},{8,2},{10,0},{12,6},{14,4},{1,11},{3,9}... | collective-permute-start | bytes 884744 | tf_op jit(solution)/shard_map/ppermute | solution.py:21
  297.3 67.5 %collective-permute-start.5 = (bf16[1,2,192,384]{3,2,1,0:T(8,128)(2,1)S(1)}, bf16[1,2,192,384]{3,2,1,0:T(8,128)(2,1)S(1)}, u32[]{:S(2)}, u32[]{:S(2)}) collective-permute-start(bf16[1,2,192,384]{3,2,1,0:T(8,128)(2,1)S(1)} %get-tuple-element.7), channel_id=1, source_target_pairs={{0,12},{2,14},{4,8},{6,10},{8,4},{10,6},{12,0},{14,2},{1,13},{3,15... | collective-permute-start | bytes 884744 | tf_op jit(solution)/shard_map/ppermute | solution.py:21
  317.3 48.2 %collective-permute-start.6 = (bf16[1,2,192,384]{3,2,1,0:T(8,128)(2,1)S(1)}, bf16[1,2,192,384]{3,2,1,0:T(8,128)(2,1)S(1)}, u32[]{:S(2)}, u32[]{:S(2)}) collective-permute-start(bf16[1,2,192,384]{3,2,1,0:T(8,128)(2,1)S(1)} %get-tuple-element.6), channel_id=1, source_target_pairs={{0,14},{2,12},{4,10},{6,8},{8,6},{10,4},{12,2},{14,0},{1,15},{3,13... | collective-permute-start | bytes 884744 | tf_op jit(solution)/shard_map/ppermute | solution.py:21
  367.9 3.5 copy-start.3
  430.6 6.0 copy-start.5
  430.6 144.6 %all-to-all-start.3 = ((bf16[8,256,1536]{2,1,0:T(8,128)(2,1)}), bf16[8,256,1536]{2,1,0:T(8,128)(2,1)}, u32[]{:S(2)}, u32[]{:S(2)}) async-start(bf16[8,256,1536]{2,1,0:T(8,128)(2,1)} %bitcast.46), calls=%async_computation.4 | async-start | bytes 12582912 | tf_op jit(solution)/shard_map/all_to_all | solution.py:86
Sparse Core Ops, SparseCore 0:
  74.4 37.3 all-gather.9
  113.9 36.0 all-gather.11
  152.1 36.0 all-gather.13
  208.9 23.5 all-gather.7
  403.0 27.5 reduce-scatter.1
